TPU v7x, 32 devices: a whole 2x2x4 slice. The times are simulated.
32 devices in a mesh: sp: 8 (over z, x), tp: 4 (over y, core).
Axes of the slice: x: 2, y: 2, z: 4, core: 2. Of those that a mesh axis runs over, the one named last changes fastest.
Arguments:
- activations: bfloat16 [6144, 2048], P('sp'), may hold values from -6 to 6
- norm_gain: bfloat16 [2048], replicated, may hold values from 0.099609375 to 1.8984375
- w_conv_outer: bfloat16 [2048, 1024], P(None, 'tp'), may hold values from -0.125 to 0.125
- w_conv_inner: bfloat16 [2048, 1024], P(None, 'tp'), may hold values from -0.125 to 0.125
- w_conv_value: bfloat16 [2048, 1024], P(None, 'tp'), may hold values from -0.125 to 0.125
- conv_taps: bfloat16 [3, 1024], P(None, 'tp'), may hold values from -3 to 3
- w_query: bfloat16 [2048, 1024], P(None, 'tp'), may hold values from -0.125 to 0.125
- w_key: bfloat16 [2048, 1024], P(None, 'tp'), may hold values from -0.125 to 0.125
- w_value: bfloat16 [2048, 1024], P(None, 'tp'), may hold values from -0.125 to 0.125
- w_gate: bfloat16 [2048, 1024], P(None, 'tp'), may hold values from -0.125 to 0.125
- log_decay: float32 [8, 6144], P('tp', 'sp'), may hold values from -2.5 to 0
- w_out_conv: bfloat16 [1024, 2048], P('tp'), may hold values from -0.125 to 0.125
- w_out_ret: bfloat16 [1024, 2048], P('tp'), may hold values from -0.125 to 0.125
Outputs:
- mixed: bfloat16 [6144, 2048], P(('sp', 'tp'))
All inputs are finite; a program needn't handle non-finite values.
Results may differ from a plain program's by a relative error of at most 0.02.
Values may be sent and summed in bfloat16 or wider, within the bound.
A program may use at most 128 MiB of HBM per device.

v0:
```python
import jax
import jax.numpy as jnp
from jax import lax
from jax.sharding import PartitionSpec as P

HEAD = 128
CONV_W = 3
BLK = 128


EPS = 1e-06


def from_behind(array, axis, by):
    size = lax.axis_size(axis)
    pairs = [(i, i + by) for i in range(size) if 0 <= i + by < size]
    return lax.ppermute(array, axis, pairs)


def for_sending(array):

    def short(part):
        return part.astype(jnp.bfloat16) if part.dtype == jnp.float32 else part

    return jax.tree.map(short, array)


def rotate_heads(block, positions):
    half_dim = block.shape[-1] // 2
    inverse = 10000.0 ** (-jnp.arange(half_dim, dtype=jnp.float32) / half_dim)
    angles = positions[:, None] * inverse[None, :]
    cosine = jnp.cos(angles)[:, None, :]
    sine_part = jnp.sin(angles)[:, None, :]
    widened = block.astype(jnp.float32)
    first = widened[..., :half_dim]
    second = widened[..., half_dim:]
    turned = jnp.concatenate(
        [first * cosine - second * sine_part, second * cosine + first * sine_part], axis=-1
    )
    return turned.astype(jnp.bfloat16)


def project(normed, weight):
    return jnp.dot(normed, weight, preferred_element_type=jnp.float32).astype(jnp.bfloat16)


def local(
    activations,
    norm_gain,
    w_conv_outer,
    w_conv_inner,
    w_conv_value,
    conv_taps,
    w_query,
    w_key,
    w_value,
    w_gate,
    log_decay,
    w_out_conv,
    w_out_ret,
):
    tok_rows = activations.shape[0]
    heads_here = log_decay.shape[0]
    blocks = tok_rows // BLK
    widened = activations.astype(jnp.float32)
    normed = (
        widened
        * lax.rsqrt(jnp.mean(widened * widened, axis=-1, keepdims=True) + EPS)
        * norm_gain.astype(jnp.float32)
    ).astype(jnp.bfloat16)
    conv_outer = project(normed, w_conv_outer)
    conv_inner = project(normed, w_conv_inner)
    conv_value = project(normed, w_conv_value)
    product = (conv_inner.astype(jnp.float32) * conv_value.astype(jnp.float32)).astype(jnp.bfloat16)
    rim = product[tok_rows - (CONV_W - 1) :]
    offset = lax.axis_index("sp") * tok_rows
    positions = (offset + jnp.arange(tok_rows, dtype=jnp.int32)).astype(jnp.float32)
    query = rotate_heads(project(normed, w_query).reshape(tok_rows, heads_here, HEAD), positions)
    key_rot = rotate_heads(project(normed, w_key).reshape(tok_rows, heads_here, HEAD), positions)
    values = project(normed, w_value)
    gate_pre = project(normed, w_gate)
    q_blocks = query.reshape(blocks, BLK, heads_here, HEAD)
    k_blocks = key_rot.reshape(blocks, BLK, heads_here, HEAD)
    v_blocks = values.reshape(blocks, BLK, heads_here, HEAD)
    levels = jnp.cumsum(log_decay.reshape(heads_here, blocks, BLK), axis=2)
    totals = levels[:, :, BLK - 1]
    scores = jnp.einsum("nihd,njhd->nhij", q_blocks, k_blocks, preferred_element_type=jnp.float32)
    level_rows = levels.transpose(1, 0, 2)
    diff = level_rows[:, :, :, None] - level_rows[:, :, None, :]
    causal = jnp.arange(BLK)[:, None] >= jnp.arange(BLK)[None, :]
    decay_tab = jnp.exp(jnp.where(causal[None, None], diff, -1e30))
    weights = (scores * decay_tab).astype(jnp.bfloat16)
    inner_part = jnp.einsum(
        "nhij,njhd->nihd", weights, v_blocks, preferred_element_type=jnp.float32
    )
    value_wide = v_blocks.astype(jnp.float32)
    key_scale = jnp.exp(totals[:, :, None] - levels).transpose(1, 2, 0)[..., None]
    key_dec = k_blocks.astype(jnp.float32) * key_scale
    contrib = jnp.einsum("njhd,njhe->nhde", key_dec, value_wide, precision=lax.Precision.HIGHEST)
    block_decay = jnp.exp(totals)
    running = jnp.zeros((heads_here, HEAD, HEAD), jnp.float32)
    before = []
    for blk_index in range(blocks):
        before.append(running)
        running = running * block_decay[:, blk_index][:, None, None] + contrib[blk_index]
    states_before = jnp.stack(before)
    query_wide = q_blocks.astype(jnp.float32)
    query_dec = query_wide * jnp.exp(levels).transpose(1, 2, 0)[..., None]
    local_cross = jnp.einsum(
        "nihd,nhde->nihe", query_dec, states_before, precision=lax.Precision.HIGHEST
    )
    device_decay = jnp.exp(jnp.sum(totals, axis=1))
    starts = jnp.cumsum(totals, axis=1) - totals
    carry_query = query_wide * jnp.exp(starts[:, :, None] + levels).transpose(1, 2, 0)[..., None]
    received, rim_wide = (
        from_behind(running.astype(jnp.bfloat16), "sp", 1).astype(running.dtype),
        from_behind(rim.astype(jnp.float32).astype(jnp.bfloat16), "sp", 1).astype(jnp.float32),
    )

    def relay_turn(turn_index, incoming_state):
        outgoing = incoming_state * device_decay[:, None, None] + running
        return from_behind(for_sending(outgoing), "sp", 1).astype(outgoing.dtype)

    incoming = lax.fori_loop(0, lax.axis_size("sp") - 2, relay_turn, received)
    rim_prev = rim_wide.astype(jnp.bfloat16)
    extended = jnp.concatenate([rim_prev, product], axis=0).astype(jnp.float32)
    taps = conv_taps.astype(jnp.float32)
    filtered = taps[0][None, :] * extended[0:tok_rows]
    for tap_index in range(1, CONV_W):
        filtered = filtered + taps[tap_index][None, :] * extended[tap_index : tap_index + tok_rows]
    conv_out = (conv_outer.astype(jnp.float32) * filtered).astype(jnp.bfloat16)
    correction = jnp.einsum(
        "nihd,hde->nihe", carry_query, incoming, precision=lax.Precision.HIGHEST
    )
    retained = inner_part + local_cross + correction
    mean_sq = jnp.mean(retained * retained, axis=-1, keepdims=True)
    gate_wide = gate_pre.reshape(blocks, BLK, heads_here, HEAD).astype(jnp.float32)
    ret_out = (retained * lax.rsqrt(mean_sq + EPS) * jax.nn.silu(gate_wide)).astype(jnp.bfloat16)
    ret_out = ret_out.reshape(tok_rows, heads_here * HEAD)
    return lax.psum_scatter(
        (
            jnp.dot(conv_out, w_out_conv, preferred_element_type=jnp.float32)
            + jnp.dot(ret_out, w_out_ret, preferred_element_type=jnp.float32)
        ).astype(jnp.bfloat16),
        "tp",
        scatter_dimension=0,
        tiled=True,
    )


def solution(mesh):
    return jax.shard_map(
        local,
        mesh=mesh,
        in_specs=(
            P("sp", None),
            P(),
            P(None, "tp"),
            P(None, "tp"),
            P(None, "tp"),
            P(None, "tp"),
            P(None, "tp"),
            P(None, "tp"),
            P(None, "tp"),
            P(None, "tp"),
            P("tp", "sp"),
            P("tp", None),
            P("tp", None),
        ),
        out_specs=P(("sp", "tp"), None),
        check_vma=False,
    )
```

profile of v0, /device:TPU:25, one launch (start us, length us, event | category | flops | bytes accessed | tf_op | source)
XLA Modules:
  0.0 171.5 jit_solution(11877780602364800260)
XLA Ops:
  6.6 2.7 %fusion = f32[768]{0:T(1024)S(1)} fusion(bf16[768,2048]{1,0:T(8,128)(2,1)} %param.15), kind=kLoop, calls=%fused_computation.3 | loop fusion | flops 4717824 | bytes 3148800 | tf_op jit(solution)/shard_map/reduce_sum | solution.py:68
  10.0 0.7 slice_reduce_fusion.5
  10.7 0.8 slice_reduce_fusion
  12.8 2.8 %fusion.2 = bf16[768,2048]{1,0:T(8,128)(2,1)S(1)} fusion(bf16[768,2048]{1,0:T(8,128)(2,1)} %param.15, f32[2048]{0:T(1024)S(1)} %convert_element_type.113, f32[768]{0:T(1024)S(1)} %add_rsqrt_fusion.1), kind=kLoop, calls=%fused_computation.5 | loop fusion | flops 6291456 | bytes 6302720 | tf_op jit(solution)/shard_map/convert_element_type | solution.py:70
  15.6 1.1 convolution_convert_fusion.1
  17.6 1.1 convolution_convert_fusion.2
  18.7 0.8 multiply_cosine_fusion
  19.5 0.9 subtract_convert_fusion.1
  21.6 3.2 %convolution_convert_fusion.3 = bf16[768,256]{1,0:T(8,128)(2,1)S(1)} fusion(bf16[768,2048]{1,0:T(8,128)(2,1)} %copy-done.1, bf16[2048,256]{1,0:T(8,128)(2,1)} %param.23), kind=kOutput, calls=%fused_computation.17 | convolution fusion | flops 805502976 | bytes 4587520 | tf_op jit(solution)/shard_map/dot_general | solution.py:44
  24.9 1.1 fusion.20
  26.1 0.7 fusion.54
  26.8 3.2 %collective-permute-start.2 = (bf16[2,128,128]{2,1,0:T(8,128)(2,1)}, bf16[2,128,128]{2,1,0:T(8,128)(2,1)}, u32[]{:S(2)}, u32[]{:S(2)}) collective-permute-start(bf16[2,128,128]{2,1,0:T(8,128)(2,1)} %get-tuple-element.45), channel_id=1, source_target_pairs={{0,4},{4,8},{8,12},{12,16},{16,20},{20,24},{24,28},{1,5},{5,9},{9,... | collective-permute-start | bytes 196616 | tf_op jit(solution)/shard_map/ppermute | solution.py:17
  30.1 3.2 %fusion.10 = f32[768,256]{1,0:T(8,128)S(1)} fusion(bf16[768,2048]{1,0:T(8,128)(2,1)} %copy-done.1, bf16[2048,256]{1,0:T(8,128)(2,1)} %param.18), kind=kOutput, calls=%fused_computation.23 | convolution fusion | flops 805699584 | bytes 4980736 | tf_op jit(solution)/shard_map/dot_general | solution.py:44
  33.3 1.0 fusion.9
  34.9 2.1 %collective-permute-start.1 = (bf16[2,256]{1,0:T(2,128)(2,1)}, bf16[2,256]{1,0:T(2,128)(2,1)}, u32[]{:S(2)}, u32[]{:S(2)}) collective-permute-start(bf16[2,256]{1,0:T(2,128)(2,1)} %slice.97), channel_id=1, source_target_pairs={{0,4},{4,8},{8,12},{12,16},{16,20},{20,24},{24,28},{1,5},{5,9},{9,... | collective-permute-start | bytes 3080 | tf_op jit(solution)/shard_map/ppermute | solution.py:17
  40.0 1.9 %concatenate.23 = bf16[6,128,2,64]{1,0,3,2:T(8,128)(2,1)} reshape(bf16[768,2,64]{0,2,1:T(8,128)(2,1)} %get-tuple-element.52) | data formatting | bytes 393216 | tf_op jit(solution)/shard_map/concatenate | solution.py:37
  41.9 1.2 copy.40
  43.1 1.3 fusion.47
  44.4 1.4 constant_dynamic-update-slice_fusion.2
  45.8 1.4 constant_dynamic-update-slice_fusion.1
  47.2 1.4 constant_dynamic-update-slice_fusion
  48.6 4.1 %fusion.6 = f32[768,256]{1,0:T(8,128)} fusion(bf16[768,2048]{1,0:T(8,128)(2,1)} %copy-done.1, bf16[2048,256]{1,0:T(8,128)(2,1)} %param.24), kind=kOutput, calls=%fused_computation.14 | convolution fusion | flops 805699584 | bytes 4980736 | tf_op jit(solution)/shard_map/dot_general | solution.py:44
  52.8 1.9 %fusion.15 = f32[6,2,128,128]{3,2,1,0:T(8,128)S(1)} fusion(f32[6,2,128,128]{3,2,1,0:T(8,128)S(1)} %add_dynamic-update-slice_fusion, f32[6,128,2]{1,2,0:T(2,128)S(1)} %copy-done.10, bf16[6,128,2,64]{3,1,2,0:T(8,128)(2,1)S(1)} %copy.40, bf16[6,128,2,64]{3,1,2,0:T(8,128)(2,1)S(1)} %copy.39), kind=kOutput, calls=%fused_computation.31 | convolution fusion | flops 302972928 | bytes 1972224 | tf_op jit(solution)/shard_map/nihd,nhde->nihe/dot_general | solution.py:109
  54.7 2.8 %fusion.3 = f32[6,128,2,128]{1,3,2,0:T(8,128)} fusion(f32[6,2,128,128]{3,2,1,0:T(8,128)S(1)} %fusion.15, f32[6,2,128]{2,1,0:T(2,128)} %copy.43, pred[128,128]{1,0:T(8,128)(4,1)S(1)} %copy-done.8, bf16[6,128,2,128]{3,2,1,0:T(2,128)(2,1)} %copy-done.3, bf16[6,128,2,64]{3,1,2,0:T(8,128)(2,1)S(1)} %copy.42, bf16[6,128,2,64]{3,1,2,0:T(8,128)(2,1)S(1)} %copy.41, ...), kind=kOutput, calls=%fused_computation.9 | convolution fusion | flops 103219200 | bytes 2775040 | tf_op jit(solution)/shard_map/nhij,njhd->nihd/dot_general | solution.py:93
  57.4 1.4 fusion.56
  58.8 1.1 exp.29
  60.0 0.7 copy.51
  60.7 1.5 reshape.137
  62.2 1.2 copy.54
  63.4 1.1 maximum_convert_fusion
  64.5 8.2 %fusion.14 = f32[768,2048]{1,0:T(8,128)} fusion(bf16[256,2048]{1,0:T(8,128)(2,1)S(1)} %copy-done, bf16[768,2048]{1,0:T(8,128)(2,1)} %copy-done.1, bf16[2048,256]{1,0:T(8,128)(2,1)} %param.17, f32[770,256]{1,0:T(8,128)S(1)} %maximum_convert_fusion, f32[256]{0:T(256)} %bitcast.107, f32[256]{0:T(256)} %bitcast.106, f32[256]{0:T(256)} %bitcast.105), kind=kOutput, calls=%fused_computation.28 | convolution fusion | flops 1612382208 | bytes 13896704 | tf_op jit(solution)/shard_map/dot_general | solution.py:142
  72.7 0.9 convert_element_type.137
  73.6 37.1 %while.10 = (s32[]{:T(128)}, f32[2,128,128]{2,1,0:T(8,128)S(1)}, f32[2]{0:T(128)S(1)}, f32[2,128,128]{2,1,0:T(8,128)S(1)}, s32[]{:T(128)}) while((s32[]{:T(128)}, f32[2,128,128]{2,1,0:T(8,128)S(1)}, f32[2]{0:T(128)S(1)}, f32[2,128,128]{2,1,0:T(8,128)S(1)}, s32[]{:T(128)}) %tuple.43), condition=%wide.region_4.5_spmd, body=%wide.region_3.4_spmd.sunk | while | flops 131074 | bytes 786541 | solution.py:124
  73.7 1.9 %collective-permute-start = (bf16[2,128,128]{2,1,0:T(8,128)(2,1)S(1)}, bf16[2,128,128]{2,1,0:T(8,128)(2,1)S(1)}, u32[]{:S(2)}, u32[]{:S(2)}) collective-permute-start(bf16[2,128,128]{2,1,0:T(8,128)(2,1)S(1)} %add_convert_fusion.6), channel_id=1, source_target_pairs={{0,4},{4,8},{8,12},{12,16},{16,20},{20,24},{24,28},{1,5},{5,9},{9,... | collective-permute-start | bytes 196616 | tf_op jit(solution)/shard_map/while/body/eval_jaxpr/ppermute | solution.py:17
  75.6 4.0 %collective-permute-done = bf16[2,128,128]{2,1,0:T(8,128)(2,1)S(1)} collective-permute-done((bf16[2,128,128]{2,1,0:T(8,128)(2,1)S(1)}, bf16[2,128,128]{2,1,0:T(8,128)(2,1)S(1)}, u32[]{:S(2)}, u32[]{:S(2)}) %collective-permute-start) | collective-permute-done | bytes 65568 | tf_op jit(solution)/shard_map/while/body/eval_jaxpr/ppermute | solution.py:17
  79.8 1.9 %collective-permute-start = (bf16[2,128,128]{2,1,0:T(8,128)(2,1)S(1)}, bf16[2,128,128]{2,1,0:T(8,128)(2,1)S(1)}, u32[]{:S(2)}, u32[]{:S(2)}) collective-permute-start(bf16[2,128,128]{2,1,0:T(8,128)(2,1)S(1)} %add_convert_fusion.6), channel_id=1, source_target_pairs={{0,4},{4,8},{8,12},{12,16},{16,20},{20,24},{24,28},{1,5},{5,9},{9,... | collective-permute-start | bytes 196616 | tf_op jit(solution)/shard_map/while/body/eval_jaxpr/ppermute | solution.py:17
  81.7 4.0 %collective-permute-done = bf16[2,128,128]{2,1,0:T(8,128)(2,1)S(1)} collective-permute-done((bf16[2,128,128]{2,1,0:T(8,128)(2,1)S(1)}, bf16[2,128,128]{2,1,0:T(8,128)(2,1)S(1)}, u32[]{:S(2)}, u32[]{:S(2)}) %collective-permute-start) | collective-permute-done | bytes 65568 | tf_op jit(solution)/shard_map/while/body/eval_jaxpr/ppermute | solution.py:17
  85.8 1.9 %collective-permute-start = (bf16[2,128,128]{2,1,0:T(8,128)(2,1)S(1)}, bf16[2,128,128]{2,1,0:T(8,128)(2,1)S(1)}, u32[]{:S(2)}, u32[]{:S(2)}) collective-permute-start(bf16[2,128,128]{2,1,0:T(8,128)(2,1)S(1)} %add_convert_fusion.6), channel_id=1, source_target_pairs={{0,4},{4,8},{8,12},{12,16},{16,20},{20,24},{24,28},{1,5},{5,9},{9,... | collective-permute-start | bytes 196616 | tf_op jit(solution)/shard_map/while/body/eval_jaxpr/ppermute | solution.py:17
  87.7 4.0 %collective-permute-done = bf16[2,128,128]{2,1,0:T(8,128)(2,1)S(1)} collective-permute-done((bf16[2,128,128]{2,1,0:T(8,128)(2,1)S(1)}, bf16[2,128,128]{2,1,0:T(8,128)(2,1)S(1)}, u32[]{:S(2)}, u32[]{:S(2)}) %collective-permute-start) | collective-permute-done | bytes 65568 | tf_op jit(solution)/shard_map/while/body/eval_jaxpr/ppermute | solution.py:17
  91.8 1.9 %collective-permute-start = (bf16[2,128,128]{2,1,0:T(8,128)(2,1)S(1)}, bf16[2,128,128]{2,1,0:T(8,128)(2,1)S(1)}, u32[]{:S(2)}, u32[]{:S(2)}) collective-permute-start(bf16[2,128,128]{2,1,0:T(8,128)(2,1)S(1)} %add_convert_fusion.6), channel_id=1, source_target_pairs={{0,4},{4,8},{8,12},{12,16},{16,20},{20,24},{24,28},{1,5},{5,9},{9,... | collective-permute-start | bytes 196616 | tf_op jit(solution)/shard_map/while/body/eval_jaxpr/ppermute | solution.py:17
  93.7 4.0 %collective-permute-done = bf16[2,128,128]{2,1,0:T(8,128)(2,1)S(1)} collective-permute-done((bf16[2,128,128]{2,1,0:T(8,128)(2,1)S(1)}, bf16[2,128,128]{2,1,0:T(8,128)(2,1)S(1)}, u32[]{:S(2)}, u32[]{:S(2)}) %collective-permute-start) | collective-permute-done | bytes 65568 | tf_op jit(solution)/shard_map/while/body/eval_jaxpr/ppermute | solution.py:17
  97.8 1.9 %collective-permute-start = (bf16[2,128,128]{2,1,0:T(8,128)(2,1)S(1)}, bf16[2,128,128]{2,1,0:T(8,128)(2,1)S(1)}, u32[]{:S(2)}, u32[]{:S(2)}) collective-permute-start(bf16[2,128,128]{2,1,0:T(8,128)(2,1)S(1)} %add_convert_fusion.6), channel_id=1, source_target_pairs={{0,4},{4,8},{8,12},{12,16},{16,20},{20,24},{24,28},{1,5},{5,9},{9,... | collective-permute-start | bytes 196616 | tf_op jit(solution)/shard_map/while/body/eval_jaxpr/ppermute | solution.py:17
  99.8 4.0 %collective-permute-done = bf16[2,128,128]{2,1,0:T(8,128)(2,1)S(1)} collective-permute-done((bf16[2,128,128]{2,1,0:T(8,128)(2,1)S(1)}, bf16[2,128,128]{2,1,0:T(8,128)(2,1)S(1)}, u32[]{:S(2)}, u32[]{:S(2)}) %collective-permute-start) | collective-permute-done | bytes 65568 | tf_op jit(solution)/shard_map/while/body/eval_jaxpr/ppermute | solution.py:17
  103.9 1.9 %collective-permute-start = (bf16[2,128,128]{2,1,0:T(8,128)(2,1)S(1)}, bf16[2,128,128]{2,1,0:T(8,128)(2,1)S(1)}, u32[]{:S(2)}, u32[]{:S(2)}) collective-permute-start(bf16[2,128,128]{2,1,0:T(8,128)(2,1)S(1)} %add_convert_fusion.6), channel_id=1, source_target_pairs={{0,4},{4,8},{8,12},{12,16},{16,20},{20,24},{24,28},{1,5},{5,9},{9,... | collective-permute-start | bytes 196616 | tf_op jit(solution)/shard_map/while/body/eval_jaxpr/ppermute | solution.py:17
  105.8 4.9 %collective-permute-done = bf16[2,128,128]{2,1,0:T(8,128)(2,1)S(1)} collective-permute-done((bf16[2,128,128]{2,1,0:T(8,128)(2,1)S(1)}, bf16[2,128,128]{2,1,0:T(8,128)(2,1)S(1)}, u32[]{:S(2)}, u32[]{:S(2)}) %collective-permute-start) | collective-permute-done | bytes 65568 | tf_op jit(solution)/shard_map/while/body/eval_jaxpr/ppermute | solution.py:17
  110.8 2.3 %multiply_reduce_fusion = (f32[6,128,2]{1,2,0:T(2,128)S(1)}, f32[6,128,2,128]{1,3,2,0:T(8,128)S(1)}) fusion(f32[6,128,2,128]{1,3,2,0:T(8,128)} %fusion.3, f32[6,128,2]{1,2,0:T(2,128)S(1)} %copy.51, bf16[6,128,2,64]{3,1,2,0:T(8,128)(2,1)S(1)} %copy.40, bf16[6,128,2,64]{3,1,2,0:T(8,128)(2,1)S(1)} %copy.39, f32[2,128,128]{2,1,0:T(8,128)S(1)} %get-tuple-element.27), kind=kOutput, calls=%fused_computation.38 | convolution fusion | flops 303561216 | bytes 2109440 | tf_op jit(solution)/shard_map/nihd,hde->nihe/dot_general | solution.py:132
  113.8 5.8 %add_convert_fusion.1 = bf16[768,2048]{1,0:T(8,128)(2,1)} fusion(f32[768,2048]{1,0:T(8,128)} %fusion.14, bf16[256,2048]{1,0:T(8,128)(2,1)} %param.27, bf16[96,8,2,128]{3,2,1,0:T(2,128)(2,1)S(1)} %bitcast.99), kind=kOutput, calls=%fused_computation.6 | convolution fusion | flops 808452096 | bytes 10878976 | tf_op jit(solution)/shard_map/dot_general | solution.py:143
  119.6 45.1 %reduce-scatter.2.cloned.1.call-done = bf16[192,2048]{1,0:T(8,128)(2,1)} async-done(((bf16[768,2048]{1,0:T(8,128)(2,1)}), bf16[192,2048]{1,0:T(8,128)(2,1)}) %reduce-scatter.2.cloned.1.call-update) | async-done | bytes 786448 | tf_op jit(solution)/shard_map/reduce_scatter | solution.py:140
  (93 shorter events, 9.1 us)
Async XLA Ops:
  6.5 57.9 %copy-start = (bf16[256,2048]{1,0:T(8,128)(2,1)S(1)}, bf16[256,2048]{1,0:T(8,128)(2,1)}, u32[]{:S(2)}) copy-start(bf16[256,2048]{1,0:T(8,128)(2,1)} %param.26) | copy-start | bytes 3145732
  6.5 2.7 %copy-start.19 = (bf16[2048]{0:T(1024)(128)(2,1)S(1)}, bf16[2048]{0:T(1024)(128)(2,1)}, u32[]{:S(2)}) copy-start(bf16[2048]{0:T(1024)(128)(2,1)} %param.16) | copy-start | bytes 12292
  6.5 2.7 %copy-start.14 = (f32[2,768]{1,0:T(2,128)S(1)}, f32[2,768]{1,0:T(2,128)}, u32[]{:S(2)}) copy-start(f32[2,768]{1,0:T(2,128)} %param.25) | copy-start | bytes 18436
  6.5 158.2 %reduce-scatter.2.cloned.1.call-start = ((), (), s32[]{:S(2)}) async-start(), calls=%async_computation.1 | async-start | bytes 3932160 | tf_op jit(solution)/shard_map/reduce_scatter | solution.py:140
  12.8 2.8 %copy-start.21 = (bf16[2048,256]{1,0:T(8,128)(2,1)S(1)}, bf16[2048,256]{1,0:T(8,128)(2,1)}, u32[]{:S(2)}) copy-start(bf16[2048,256]{1,0:T(8,128)(2,1)} %param.22) | copy-start | bytes 3145732
  15.5 1.7 copy-start.1
  15.5 2.0 %copy-start.22 = (bf16[2048,256]{1,0:T(8,128)(2,1)S(1)}, bf16[2048,256]{1,0:T(8,128)(2,1)}, u32[]{:S(2)}) copy-start(bf16[2048,256]{1,0:T(8,128)(2,1)} %param.21) | copy-start | bytes 3145732
  21.5 3.3 %copy-start.9 = (f32[6,128,2]{1,2,0:T(2,128)S(1)}, f32[6,128,2]{1,2,0:T(2,128)}, u32[]{:S(2)}) copy-start(f32[6,128,2]{1,2,0:T(2,128)} %copy.46) | copy-start | bytes 18436
  21.5 4.5 %copy-start.12 = (f32[2]{0:T(128)S(1)}, f32[2]{0:T(128)}, u32[]{:S(2)}) copy-start(f32[2]{0:T(128)} %get-tuple-element.34) | copy-start | bytes 28
  21.5 4.5 %copy-start.13 = (f32[2]{0:T(128)S(1)}, f32[2]{0:T(128)}, u32[]{:S(2)}) copy-start(f32[2]{0:T(128)} %get-tuple-element.36) | copy-start | bytes 28
  21.5 4.5 %copy-start.15 = (f32[2]{0:T(128)S(1)}, f32[2]{0:T(128)}, u32[]{:S(2)}) copy-start(f32[2]{0:T(128)} %get-tuple-element.32) | copy-start | bytes 28
  21.5 4.5 %copy-start.17 = (f32[2]{0:T(128)S(1)}, f32[2]{0:T(128)}, u32[]{:S(2)}) copy-start(f32[2]{0:T(128)} %get-tuple-element.33) | copy-start | bytes 28
  21.6 4.5 %copy-start.18 = (f32[2]{0:T(128)S(1)}, f32[2]{0:T(128)}, u32[]{:S(2)}) copy-start(f32[2]{0:T(128)} %get-tuple-element.35) | copy-start | bytes 28
  21.6 4.5 %copy-start.20 = (f32[2]{0:T(128)S(1)}, f32[2]{0:T(128)}, u32[]{:S(2)}) copy-start(f32[2]{0:T(128)} %get-tuple-element.31) | copy-start | bytes 28
  24.8 1.1 copy-start.3
  26.1 7.2 %copy-start.2 = (bf16[768,2048]{1,0:T(8,128)(2,1)S(1)}, bf16[768,2048]{1,0:T(8,128)(2,1)}, u32[]{:S(2)}) copy-start(bf16[768,2048]{1,0:T(8,128)(2,1)} %copy-done.1) | copy-start | bytes 9437188
  26.1 7.2 %copy-start.23 = (bf16[2048,256]{1,0:T(8,128)(2,1)S(1)}, bf16[2048,256]{1,0:T(8,128)(2,1)}, u32[]{:S(2)}) copy-start(bf16[2048,256]{1,0:T(8,128)(2,1)} %param.19) | copy-start | bytes 3145732
  26.8 45.8 %collective-permute-start.2 = (bf16[2,128,128]{2,1,0:T(8,128)(2,1)}, bf16[2,128,128]{2,1,0:T(8,128)(2,1)}, u32[]{:S(2)}, u32[]{:S(2)}) collective-permute-start(bf16[2,128,128]{2,1,0:T(8,128)(2,1)} %get-tuple-element.45), channel_id=1, source_target_pairs={{0,4},{4,8},{8,12},{12,16},{16,20},{20,24},{24,28},{1,5},{5,9},{9,... | collective-permute-start | bytes 196616 | tf_op jit(solution)/shard_map/ppermute | solution.py:17
  33.3 6.2 %copy-start.6 = (bf16[768,2,64]{0,2,1:T(8,128)(2,1)S(1)}, bf16[768,2,64]{0,2,1:T(8,128)(2,1)}, u32[]{:S(2)}) copy-start(bf16[768,2,64]{0,2,1:T(8,128)(2,1)} %get-tuple-element.51) | copy-start | bytes 589828
  34.3 5.2 %copy-start.7 = (bf16[768,256]{1,0:T(8,128)(2,1)}, bf16[768,256]{1,0:T(8,128)(2,1)S(1)}, u32[]{:S(2)}) copy-start(bf16[768,256]{1,0:T(8,128)(2,1)S(1)} %fusion.9) | copy-start | bytes 1179652
  34.9 28.4 %collective-permute-start.1 = (bf16[2,256]{1,0:T(2,128)(2,1)}, bf16[2,256]{1,0:T(2,128)(2,1)}, u32[]{:S(2)}, u32[]{:S(2)}) collective-permute-start(bf16[2,256]{1,0:T(2,128)(2,1)} %slice.97), channel_id=1, source_target_pairs={{0,4},{4,8},{8,12},{12,16},{16,20},{20,24},{24,28},{1,5},{5,9},{9,... | collective-permute-start | bytes 3080 | tf_op jit(solution)/shard_map/ppermute | solution.py:17
  47.2 5.5 %copy-start.16 = (f32[2]{0:T(128)S(1)}, f32[2]{0:T(128)}, u32[]{:S(2)}) copy-start(f32[2]{0:T(128)} %get-tuple-element.32) | copy-start | bytes 28
  48.6 4.1 %copy-start.5 = (f32[6,2,128,128]{3,2,1,0:T(8,128)S(1)}, f32[6,2,128,128]{3,2,1,0:T(8,128)}, u32[]{:S(2)}) copy-start(f32[6,2,128,128]{3,2,1,0:T(8,128)} %get-tuple-element.47) | copy-start | bytes 2359300
  48.6 4.2 %copy-start.10 = (f32[6,128,2]{1,2,0:T(2,128)S(1)}, f32[6,128,2]{1,2,0:T(2,128)}, u32[]{:S(2)}) copy-start(f32[6,128,2]{1,2,0:T(2,128)} %copy.49) | copy-start | bytes 18436
  48.6 6.1 %copy-start.8 = (pred[128,128]{1,0:T(8,128)(4,1)S(1)}, pred[128,128]{1,0:T(8,128)(4,1)}, u32[]{:S(2)}) copy-start(pred[128,128]{1,0:T(8,128)(4,1)} %iota_compare_fusion) | copy-start | bytes 49156
  64.4 9.2 %copy-start.11 = (f32[2]{0:T(128)S(1)}, f32[2]{0:T(128)}, u32[]{:S(2)}) copy-start(f32[2]{0:T(128)} %exp.29) | copy-start | bytes 28
  72.7 40.5 %copy-start.4 = (f32[6,128,2,128]{1,3,2,0:T(8,128)S(1)}, f32[6,128,2,128]{1,3,2,0:T(8,128)}, u32[]{:S(2)}) copy-start(f32[6,128,2,128]{1,3,2,0:T(8,128)} %copy.54) | copy-start | bytes 2359300
  73.7 5.9 %collective-permute-start = (bf16[2,128,128]{2,1,0:T(8,128)(2,1)S(1)}, bf16[2,128,128]{2,1,0:T(8,128)(2,1)S(1)}, u32[]{:S(2)}, u32[]{:S(2)}) collective-permute-start(bf16[2,128,128]{2,1,0:T(8,128)(2,1)S(1)} %add_convert_fusion.6), channel_id=1, source_target_pairs={{0,4},{4,8},{8,12},{12,16},{16,20},{20,24},{24,28},{1,5},{5,9},{9,... | collective-permute-start | bytes 196616 | tf_op jit(solution)/shard_map/while/body/eval_jaxpr/ppermute | solution.py:17
  79.8 5.9 %collective-permute-start = (bf16[2,128,128]{2,1,0:T(8,128)(2,1)S(1)}, bf16[2,128,128]{2,1,0:T(8,128)(2,1)S(1)}, u32[]{:S(2)}, u32[]{:S(2)}) collective-permute-start(bf16[2,128,128]{2,1,0:T(8,128)(2,1)S(1)} %add_convert_fusion.6), channel_id=1, source_target_pairs={{0,4},{4,8},{8,12},{12,16},{16,20},{20,24},{24,28},{1,5},{5,9},{9,... | collective-permute-start | bytes 196616 | tf_op jit(solution)/shard_map/while/body/eval_jaxpr/ppermute | solution.py:17
  85.8 5.9 %collective-permute-start = (bf16[2,128,128]{2,1,0:T(8,128)(2,1)S(1)}, bf16[2,128,128]{2,1,0:T(8,128)(2,1)S(1)}, u32[]{:S(2)}, u32[]{:S(2)}) collective-permute-start(bf16[2,128,128]{2,1,0:T(8,128)(2,1)S(1)} %add_convert_fusion.6), channel_id=1, source_target_pairs={{0,4},{4,8},{8,12},{12,16},{16,20},{20,24},{24,28},{1,5},{5,9},{9,... | collective-permute-start | bytes 196616 | tf_op jit(solution)/shard_map/while/body/eval_jaxpr/ppermute | solution.py:17
  91.8 5.9 %collective-permute-start = (bf16[2,128,128]{2,1,0:T(8,128)(2,1)S(1)}, bf16[2,128,128]{2,1,0:T(8,128)(2,1)S(1)}, u32[]{:S(2)}, u32[]{:S(2)}) collective-permute-start(bf16[2,128,128]{2,1,0:T(8,128)(2,1)S(1)} %add_convert_fusion.6), channel_id=1, source_target_pairs={{0,4},{4,8},{8,12},{12,16},{16,20},{20,24},{24,28},{1,5},{5,9},{9,... | collective-permute-start | bytes 196616 | tf_op jit(solution)/shard_map/while/body/eval_jaxpr/ppermute | solution.py:17
  97.8 5.9 %collective-permute-start = (bf16[2,128,128]{2,1,0:T(8,128)(2,1)S(1)}, bf16[2,128,128]{2,1,0:T(8,128)(2,1)S(1)}, u32[]{:S(2)}, u32[]{:S(2)}) collective-permute-start(bf16[2,128,128]{2,1,0:T(8,128)(2,1)S(1)} %add_convert_fusion.6), channel_id=1, source_target_pairs={{0,4},{4,8},{8,12},{12,16},{16,20},{20,24},{24,28},{1,5},{5,9},{9,... | collective-permute-start | bytes 196616 | tf_op jit(solution)/shard_map/while/body/eval_jaxpr/ppermute | solution.py:17
  103.9 6.9 %collective-permute-start = (bf16[2,128,128]{2,1,0:T(8,128)(2,1)S(1)}, bf16[2,128,128]{2,1,0:T(8,128)(2,1)S(1)}, u32[]{:S(2)}, u32[]{:S(2)}) collective-permute-start(bf16[2,128,128]{2,1,0:T(8,128)(2,1)S(1)} %add_convert_fusion.6), channel_id=1, source_target_pairs={{0,4},{4,8},{8,12},{12,16},{16,20},{20,24},{24,28},{1,5},{5,9},{9,... | collective-permute-start | bytes 196616 | tf_op jit(solution)/shard_map/while/body/eval_jaxpr/ppermute | solution.py:17
Sparse Core Ops, SparseCore 0:
  119.7 44.9 reduce-scatter.1
where the time goes:
time: 174 us; the launch traced here: 172 us
  waiting for transfers between devices  69.9 us (40%)
  matrix products  35.8 us (21%)
  other arithmetic  19.8 us (11%)
  starting transfers between devices  16.9 us (10%)
  local copies, waits for them, and re-layouts  15.1 us (9%)
  between operations  13.9 us (8%)
    reduce_scatter x1, waiting for transfers between devices, local(): lax.psum_scatter((jnp.dot(conv_out, w_out_conv, preferred_element_type=jn...  45.1 us
    ppermute x8, waiting for transfers between devices, from_behind(): return lax.ppermute(array, axis, pairs)  24.9 us
    ppermute x8, starting transfers between devices, from_behind(): return lax.ppermute(array, axis, pairs)  16.9 us
    dot_general x6, matrix products, project(): jnp.dot(normed, weight, preferred_element_type=jnp.float32)  13.6 us
    dot_general x1, matrix products, local(): jnp.dot(conv_out, w_out_conv, preferred_element_type=jnp.float32)  8.22 us
    dot_general x1, matrix products, local(): jnp.dot(ret_out, w_out_ret, preferred_element_type=jnp.float32)  5.81 us
    unnamed x4, other arithmetic  5.5 us
    concatenate x8, local copies, waits for them, and re-layouts, rotate_heads(): jnp.concatenate([first * cosine - second * sine_part, second * cosine + f...  4.65 us
  transfers between devices with their start and end apart: 9, of which 7 were waited for; matrix products, arithmetic and copies ran while one was open for 24% of the time, Pallas kernels for 0%

commit v1 on v0

v1 whole, which is shorter than its diff:
```python
import functools

import jax
import jax.numpy as jnp
import numpy as np
from jax import lax
from jax.experimental import pallas as pl
from jax.experimental.pallas import tpu as pltpu
from jax.sharding import PartitionSpec as P

HEAD = 128
CONV_W = 3
BLK = 128
EPS = 1e-06
MESH = pl.DeviceIdType.MESH
F32 = jnp.float32
BF16 = jnp.bfloat16
HI = lax.Precision.HIGHEST


def windows_of(size):
    widths, width = [], 1
    while width < size:
        widths.append(width)
        width *= 3
    return widths


def rotary_tables(total_blocks):
    half = HEAD // 2
    inverse = 10000.0 ** (-np.arange(half, dtype=np.float64) / half)
    sign = np.concatenate([-np.ones(half), np.ones(half)])

    def table(positions):
        angles = positions[:, None] * np.concatenate([inverse, inverse])[None, :]
        return np.cos(angles).astype(np.float32), (np.sin(angles) * sign).astype(np.float32)

    return table(np.arange(BLK, dtype=np.float64)) + table(
        np.arange(total_blocks, dtype=np.float64) * BLK
    )


def kernel(
    n_sp,
    chunks,
    acts_hbm,
    gain_ref,
    wco_hbm,
    wci_hbm,
    wcv_hbm,
    taps_ref,
    wq_hbm,
    wk_hbm,
    wv_hbm,
    wg_hbm,
    decay_ref,
    woc_hbm,
    wor_hbm,
    cos_in_ref,
    sin_in_ref,
    cos_off_ref,
    sin_off_ref,
    out_ref,
    x_ref,
    w_ref,
    wo_ref,
    k_ref,
    v_ref,
    q_ref,
    g_ref,
    co_ref,
    ext_ref,
    inner_ref,
    mix_ref,
    st_ref,
    cs_ref,
    sn_ref,
    ld_ref,
    run_ref,
    es_ref,
    el_ref,
    send_s,
    send_l,
    recv_s,
    recv_l,
    send_a,
    recv_a,
    own_ref,
    send_b,
    recv_b,
    x_sem,
    w_sem,
    scan_send_sem,
    scan_recv_sem,
    rim_sem,
    a_sem,
    b_sem,
):
    sp = lax.axis_index("sp")
    tp = lax.axis_index("tp")
    rows, width = x_ref.shape
    heads = decay_ref.shape[0]
    ch = co_ref.shape[1]
    rc = heads * HEAD
    blocks = rows // BLK
    tiles = blocks
    proj = 256 if rows % 256 == 0 else BLK
    widths = windows_of(n_sp)
    distances = [d for w in widths for d in (w, 2 * w) if d < n_sp]
    sibling, across = tp ^ 1, tp ^ 2

    x_copies = [
        pltpu.make_async_copy(
            acts_hbm.at[pl.ds(i * BLK, BLK)], x_ref.at[pl.ds(i * BLK, BLK)], x_sem.at[i]
        )
        for i in range(tiles)
    ]
    bounds, w_copies = {}, {}
    start = 0
    for index, (name, ref) in enumerate(
        (
            ("k", wk_hbm),
            ("v", wv_hbm),
            ("q", wq_hbm),
            ("g", wg_hbm),
            ("ci", wci_hbm),
            ("cv", wcv_hbm),
            ("co", wco_hbm),
        )
    ):
        size = ref.shape[1]
        bounds[name] = (start, start + size)
        w_copies[name] = pltpu.make_async_copy(
            ref, w_ref.at[:, pl.ds(start, size)], w_sem.at[index]
        )
        start += size
    w_copies["oc"] = pltpu.make_async_copy(woc_hbm, wo_ref.at[pl.ds(0, ch)], w_sem.at[7])
    w_copies["or"] = pltpu.make_async_copy(wor_hbm, wo_ref.at[pl.ds(ch, rc)], w_sem.at[8])
    for copy in x_copies:
        copy.start()
    for name in ("k", "v", "q", "g", "ci", "cv", "co", "oc", "or"):
        w_copies[name].start()

    barrier = pltpu.get_barrier_semaphore()
    expected = jnp.int32(2)
    for peer in (sibling, across):
        pl.semaphore_signal(barrier, inc=1, device_id=(sp, peer), device_id_type=MESH)
    for d in distances:
        @pl.when(sp + d < n_sp)
        def _(d=d):
            pl.semaphore_signal(barrier, inc=1, device_id=(sp + d, tp), device_id_type=MESH)

        @pl.when(sp >= d)
        def _(d=d):
            pl.semaphore_signal(barrier, inc=1, device_id=(sp - d, tp), device_id_type=MESH)

        expected = (
            expected
            + jnp.where(sp + d < n_sp, jnp.int32(1), jnp.int32(0))
            + jnp.where(sp >= d, jnp.int32(1), jnp.int32(0))
        )

    for b in range(blocks):
        c_off = cos_off_ref[pl.ds(sp * blocks + b, 1), :]
        s_off = sin_off_ref[pl.ds(sp * blocks + b, 1), :]
        c_in, s_in = cos_in_ref[...], sin_in_ref[...]
        cs_ref[pl.ds(b * BLK, BLK), :] = c_off * c_in - s_off * s_in
        sn_ref[pl.ds(b * BLK, BLK), :] = s_off * c_in + c_off * s_in

    ld_ref[...] = jnp.zeros_like(ld_ref)
    for h in range(heads):
        for b in range(blocks):
            j = h * blocks + b
            ld_ref[j : j + 1, :] = decay_ref[h : h + 1, b * BLK : (b + 1) * BLK]
    ld = ld_ref[...]
    row_i = lax.broadcasted_iota(jnp.int32, (BLK, BLK), 0)
    col_i = lax.broadcasted_iota(jnp.int32, (BLK, BLK), 1)
    causal = row_i >= col_i
    upper = jnp.where(row_i <= col_i, 1.0, 0.0).astype(F32)
    lower = jnp.where(row_i >= col_i, 1.0, 0.0).astype(F32)
    after = jnp.where(row_i < col_i, 1.0, 0.0).astype(F32)
    ones = jnp.ones((BLK, BLK), F32)
    nt = (((1,), (1,)), ((), ()))
    level_row = jnp.dot(ld, upper, precision=HI, preferred_element_type=F32)
    total_row = jnp.dot(ld, ones, precision=HI, preferred_element_type=F32)
    level_col = lax.dot_general(lower, ld, nt, precision=HI, preferred_element_type=F32)
    rest_col = lax.dot_general(after, ld, nt, precision=HI, preferred_element_type=F32)
    key_scale = jnp.exp(rest_col)
    query_scale = jnp.exp(level_col)

    def norm_tile(i, carry):
        at = pl.ds(pl.multiple_of(i * BLK, BLK), BLK)
        pltpu.make_async_copy(acts_hbm.at[at], x_ref.at[at], x_sem.at[i]).wait()
        x = x_ref[at, :].astype(F32)
        mean_sq = jnp.mean(x * x, axis=-1, keepdims=True)
        x_ref[at, :] = (x * lax.rsqrt(mean_sq + EPS) * gain_ref[...].astype(F32)).astype(BF16)
        return carry

    lax.fori_loop(0, tiles, norm_tile, 0)

    def project(at, first, last):
        lo, hi = bounds[first][0], bounds[last][1]
        return jnp.dot(x_ref[at, :], w_ref[:, lo:hi], preferred_element_type=F32).astype(BF16)

    def rotate(part, at):
        cosine, sine = cs_ref[at, :], sn_ref[at, :]
        turned = []
        for h in range(heads):
            wide = part[:, h * HEAD : (h + 1) * HEAD].astype(F32)
            turned.append((wide * cosine + pltpu.roll(wide, HEAD // 2, 1) * sine).astype(BF16))
        return turned

    def tile_at(i):
        return pl.ds(pl.multiple_of(i * proj, proj), proj)

    w_copies["k"].wait()
    w_copies["v"].wait()

    def kv_tile(i, carry):
        at = tile_at(i)
        both = project(at, "k", "v")
        v_ref[at, :] = both[:, rc:]
        for h, turned in enumerate(rotate(both[:, :rc], at)):
            k_ref[at, h * HEAD : (h + 1) * HEAD] = turned
        return carry

    lax.fori_loop(0, rows // proj, kv_tile, 0)

    device_total = []
    starts = []
    for h in range(heads):
        running = jnp.zeros((HEAD, HEAD), F32)
        total = jnp.zeros((1, HEAD), F32)
        cols = slice(h * HEAD, (h + 1) * HEAD)
        for b in range(blocks):
            j = h * blocks + b
            st_ref[j] = running
            starts.append(total)
            at = slice(b * BLK, (b + 1) * BLK)
            k_dec = (k_ref[at, cols].astype(F32) * key_scale[:, j : j + 1]).astype(BF16)
            contrib = lax.dot_general(
                k_dec, v_ref[at, cols], (((0,), (0,)), ((), ())), preferred_element_type=F32
            )
            running = running * jnp.exp(total_row[j : j + 1, :]) + contrib
            total = total + total_row[j : j + 1, :]
        run_ref[cols, :] = running
        device_total.append(total)

    pl.semaphore_wait(barrier, expected)

    es_ref[...] = jnp.zeros_like(es_ref)
    el_ref[...] = jnp.zeros_like(el_ref)
    send_l[...] = jnp.zeros_like(send_l)

    def scan_copies(r, j, d):
        to = (sp + d, tp)
        return (
            pltpu.make_async_remote_copy(
                src_ref=send_s.at[r],
                dst_ref=recv_s.at[r, j],
                send_sem=scan_send_sem.at[r, j, 0],
                recv_sem=scan_recv_sem.at[r, j, 0],
                device_id=to,
                device_id_type=MESH,
            ),
            pltpu.make_async_remote_copy(
                src_ref=send_l.at[r],
                dst_ref=recv_l.at[r, j],
                send_sem=scan_send_sem.at[r, j, 1],
                recv_sem=scan_recv_sem.at[r, j, 1],
                device_id=to,
                device_id_type=MESH,
            ),
        )

    def scan_send(r):
        for h in range(heads):
            cols = slice(h * HEAD, (h + 1) * HEAD)
            state = run_ref[cols, :]
            if r > 0:
                state = state + jnp.exp(device_total[h]) * es_ref[cols, :]
            send_s[r, cols, :] = state.astype(BF16)
            send_l[r, h : h + 1, :] = device_total[h] + el_ref[h : h + 1, :]
        for j in range(2):
            d = (j + 1) * widths[r]
            if d < n_sp:
                @pl.when(sp + d < n_sp)
                def _(j=j, d=d):
                    for copy in scan_copies(r, j, d):
                        copy.start()

    def scan_receive(r):
        for j in range(2):
            d = (j + 1) * widths[r]
            if d < n_sp:
                @pl.when(sp >= d)
                def _(j=j, d=d):
                    for copy in scan_copies(r, j, d):
                        copy.wait_recv()
                    for h in range(heads):
                        cols = slice(h * HEAD, (h + 1) * HEAD)
                        es_ref[cols, :] += jnp.exp(el_ref[h : h + 1, :]) * recv_s[
                            r, j, cols, :
                        ].astype(F32)
                    el_ref[...] += recv_l[r, j]

    scan_send(0)

    w_copies["q"].wait()
    w_copies["g"].wait()

    def qg_tile(i, carry):
        at = tile_at(i)
        both = project(at, "q", "g")
        g_ref[at, :] = both[:, rc:]
        for h, turned in enumerate(rotate(both[:, :rc], at)):
            q_ref[at, h * HEAD : (h + 1) * HEAD] = turned
        return carry

    lax.fori_loop(0, rows // proj, qg_tile, 0)

    for r in range(1, len(widths)):
        scan_receive(r - 1)
        scan_send(r)

    for name in ("ci", "cv", "co"):
        w_copies[name].wait()

    def conv_tile(i, carry):
        at = tile_at(i)
        three = project(at, "ci", "co")
        product = (three[:, :ch].astype(F32) * three[:, ch : 2 * ch].astype(F32)).astype(BF16)
        ext_ref[pl.ds(pl.multiple_of(i * proj + 8, 8), proj), :] = product.astype(F32)
        co_ref[at, :] = three[:, 2 * ch :]
        return carry

    lax.fori_loop(0, rows // proj, conv_tile, 0)

    rim = pltpu.make_async_remote_copy(
        src_ref=ext_ref.at[pl.ds(rows, 8)],
        dst_ref=ext_ref.at[pl.ds(0, 8)],
        send_sem=rim_sem.at[0],
        recv_sem=rim_sem.at[1],
        device_id=(sp + 1, tp),
        device_id_type=MESH,
    )

    @pl.when(sp == 0)
    def _():
        ext_ref[pl.ds(0, 8), :] = jnp.zeros((8, ch), F32)

    @pl.when(sp + 1 < n_sp)
    def _():
        rim.start()

    for h in range(heads):
        cols = slice(h * HEAD, (h + 1) * HEAD)
        for b in range(blocks):
            j = h * blocks + b
            at = slice(b * BLK, (b + 1) * BLK)
            scores = lax.dot_general(q_ref[at, cols], k_ref[at, cols], nt, preferred_element_type=F32)
            diff = level_col[:, j : j + 1] - level_row[j : j + 1, :]
            weights = (scores * jnp.exp(jnp.where(causal, diff, -1e30))).astype(BF16)
            inner_ref[at, cols] = jnp.dot(weights, v_ref[at, cols], preferred_element_type=F32)

    @pl.when(sp >= 1)
    def _():
        rim.wait_recv()

    taps = taps_ref[...].astype(F32)
    for b in range(blocks):
        at = slice(b * BLK, (b + 1) * BLK)
        base = b * BLK + 8 - (CONV_W - 1)
        filtered = taps[0:1, :] * ext_ref[base : base + BLK, :]
        for t in range(1, CONV_W):
            filtered = filtered + taps[t : t + 1, :] * ext_ref[base + t : base + t + BLK, :]
        mix_ref[at, 0:ch] = (co_ref[at, :].astype(F32) * filtered).astype(BF16)

    scan_receive(len(widths) - 1)

    for b in range(blocks):
        at = slice(b * BLK, (b + 1) * BLK)
        for h in range(heads):
            cols = slice(h * HEAD, (h + 1) * HEAD)
            j = h * blocks + b
            state = (st_ref[j] + jnp.exp(starts[j]) * es_ref[cols, :]).astype(BF16)
            q_dec = (q_ref[at, cols].astype(F32) * query_scale[:, j : j + 1]).astype(BF16)
            retained = inner_ref[at, cols] + jnp.dot(q_dec, state, preferred_element_type=F32)
            mean_sq = jnp.mean(retained * retained, axis=-1, keepdims=True)
            gate = g_ref[at, cols].astype(F32)
            gate = gate / (1.0 + jnp.exp(-gate))
            mix_ref[at, ch + h * HEAD : ch + (h + 1) * HEAD] = (
                retained * lax.rsqrt(mean_sq + EPS) * gate
            ).astype(BF16)

    w_copies["oc"].wait()
    w_copies["or"].wait()
    part = out_ref.shape[0]
    wide = width // chunks

    def partial(block, c):
        at = pl.ds(pl.multiple_of(block * part, 16), part)
        return jnp.dot(
            mix_ref[at, :], wo_ref[:, c * wide : (c + 1) * wide], preferred_element_type=F32
        )

    def to_sibling(p, c):
        return pltpu.make_async_remote_copy(
            src_ref=send_a.at[p, c],
            dst_ref=recv_a.at[p, c],
            send_sem=a_sem.at[0, p, c],
            recv_sem=a_sem.at[1, p, c],
            device_id=(sp, sibling),
            device_id_type=MESH,
        )

    def to_across(c):
        return pltpu.make_async_remote_copy(
            src_ref=send_b.at[c],
            dst_ref=recv_b.at[c],
            send_sem=b_sem.at[0, c],
            recv_sem=b_sem.at[1, c],
            device_id=(sp, across),
            device_id_type=MESH,
        )

    def send_sibling(p, c):
        send_a[p, c] = partial(tp ^ (3 if p == 0 else 1), c).astype(BF16)
        to_sibling(p, c).start()

    def send_across(c):
        own = partial(across, c)
        to_sibling(0, c).wait_recv()
        send_b[c] = (own + recv_a[0, c].astype(F32)).astype(BF16)
        to_across(c).start()

    send_sibling(0, 0)
    for c in range(chunks):
        if c + 1 < chunks:
            send_sibling(0, c + 1)
        send_across(c)
    for c in range(chunks):
        send_sibling(1, c)
    for c in range(chunks):
        own_ref[c] = partial(tp, c)
    for c in range(chunks):
        to_sibling(1, c).wait_recv()
        own_ref[c] += recv_a[1, c].astype(F32)
    for c in range(chunks):
        to_across(c).wait_recv()
        out_ref[:, c * wide : (c + 1) * wide] = (own_ref[c] + recv_b[c].astype(F32)).astype(BF16)

    for r in range(len(widths)):
        for j in range(2):
            d = (j + 1) * widths[r]
            if d < n_sp:
                @pl.when(sp + d < n_sp)
                def _(r=r, j=j, d=d):
                    for copy in scan_copies(r, j, d):
                        copy.wait_send()

    @pl.when(sp + 1 < n_sp)
    def _():
        rim.wait_send()

    for c in range(chunks):
        to_sibling(0, c).wait_send()
        to_sibling(1, c).wait_send()
        to_across(c).wait_send()


def local(
    n_sp,
    n_tp,
    activations,
    norm_gain,
    w_conv_outer,
    w_conv_inner,
    w_conv_value,
    conv_taps,
    w_query,
    w_key,
    w_value,
    w_gate,
    log_decay,
    w_out_conv,
    w_out_ret,
):
    rows, width = activations.shape
    heads = log_decay.shape[0]
    blocks = rows // BLK
    ch = w_conv_outer.shape[1]
    rc = heads * HEAD
    part = rows // n_tp
    chunks = 4
    wide = width // chunks
    rounds = len(windows_of(n_sp))
    pad = -(-heads * blocks // 8) * 8
    tables = [jnp.asarray(t) for t in rotary_tables(n_sp * blocks)]
    vmem = pl.BlockSpec(memory_space=pltpu.VMEM)
    hbm = pl.BlockSpec(memory_space=pl.ANY)
    dma = pltpu.SemaphoreType.DMA
    return pl.pallas_call(
        functools.partial(kernel, n_sp, chunks),
        out_shape=jax.ShapeDtypeStruct((part, width), BF16),
        in_specs=[hbm, vmem, hbm, hbm, hbm, vmem, hbm, hbm, hbm, hbm, vmem, hbm, hbm] + [vmem] * 4,
        out_specs=vmem,
        scratch_shapes=[
            pltpu.VMEM((rows, width), BF16),
            pltpu.VMEM((width, 3 * ch + 4 * rc), BF16),
            pltpu.VMEM((ch + rc, width), BF16),
            pltpu.VMEM((rows, rc), BF16),
            pltpu.VMEM((rows, rc), BF16),
            pltpu.VMEM((rows, rc), BF16),
            pltpu.VMEM((rows, rc), BF16),
            pltpu.VMEM((rows, ch), BF16),
            pltpu.VMEM((rows + 8, ch), F32),
            pltpu.VMEM((rows, rc), F32),
            pltpu.VMEM((rows, ch + rc), BF16),
            pltpu.VMEM((heads * blocks, HEAD, HEAD), F32),
            pltpu.VMEM((rows, HEAD), F32),
            pltpu.VMEM((rows, HEAD), F32),
            pltpu.VMEM((pad, BLK), F32),
            pltpu.VMEM((rc, HEAD), F32),
            pltpu.VMEM((rc, HEAD), F32),
            pltpu.VMEM((8, HEAD), F32),
            pltpu.VMEM((rounds, rc, HEAD), BF16),
            pltpu.VMEM((rounds, 8, HEAD), F32),
            pltpu.VMEM((rounds, 2, rc, HEAD), BF16),
            pltpu.VMEM((rounds, 2, 8, HEAD), F32),
            pltpu.VMEM((2, chunks, part, wide), BF16),
            pltpu.VMEM((2, chunks, part, wide), BF16),
            pltpu.VMEM((chunks, part, wide), F32),
            pltpu.VMEM((chunks, part, wide), BF16),
            pltpu.VMEM((chunks, part, wide), BF16),
            dma((blocks,)),
            dma((9,)),
            dma((rounds, 2, 2)),
            dma((rounds, 2, 2)),
            dma((2,)),
            dma((2, 2, chunks)),
            dma((2, chunks)),
        ],
        compiler_params=pltpu.CompilerParams(
            collective_id=0, has_side_effects=True, vmem_limit_bytes=60 * 1024 * 1024
        ),
    )(
        activations,
        norm_gain.reshape(1, width),
        w_conv_outer,
        w_conv_inner,
        w_conv_value,
        conv_taps,
        w_query,
        w_key,
        w_value,
        w_gate,
        log_decay,
        w_out_conv,
        w_out_ret,
        *tables,
    )


def solution(mesh):
    return jax.shard_map(
        functools.partial(local, mesh.shape["sp"], mesh.shape["tp"]),
        mesh=mesh,
        in_specs=(
            P("sp", None),
            P(),
            P(None, "tp"),
            P(None, "tp"),
            P(None, "tp"),
            P(None, "tp"),
            P(None, "tp"),
            P(None, "tp"),
            P(None, "tp"),
            P(None, "tp"),
            P("tp", "sp"),
            P("tp", None),
            P("tp", None),
        ),
        out_specs=P(("sp", "tp"), None),
        check_vma=False,
    )
```

time: 174 us -> 49.6 us (0.29); the launches traced: 172 us -> 49.4 us
  waiting for transfers between devices: 69.9 us -> 0 us
  Pallas kernels: 0 us -> 46 us
  matrix products: 35.8 us -> 0 us
  other arithmetic: 19.8 us -> 0 us
  starting transfers between devices: 16.9 us -> 0 us
  between operations: 13.9 us -> 0.01 us
  local copies, waits for them, and re-layouts: 15.1 us -> 3.38 us
    pallas_call x0 -> x1, Pallas kernels: none -> 46 us  [local(): pl.pallas_call(functools.partial(kernel, n_sp, chunks), out_shape=jax.Sha...]
    reduce_scatter x1 -> x0, waiting for transfers between devices: 45.1 us -> none  [local(): lax.psum_scatter((jnp.dot(conv_out, w_out_conv, preferred_element_type=jn...]
    dot_general x12 -> x0, matrix products: 35.8 us -> none  [the longest x6 13.6 us: project(): jnp.dot(normed, weight, preferred_element_type=jnp.float32)]
    ppermute x8 -> x0, waiting for transfers between devices: 24.9 us -> none  [from_behind(): return lax.ppermute(array, axis, pairs)]
    ppermute x8 -> x0, starting transfers between devices: 16.9 us -> none  [from_behind(): return lax.ppermute(array, axis, pairs)]
    convert_element_type x21 -> x0, other arithmetic: 6.42 us -> none  [the longest x1 2.75 us: local(): normed = (widened * lax.rsqrt(jnp.mean(widened * widened, axis=-1, keepdi...]
    unnamed x4 -> x0, other arithmetic: 5.5 us -> none
    concatenate x8 -> x0, local copies, waits for them, and re-layouts: 4.65 us -> none  [rotate_heads(): jnp.concatenate([first * cosine - second * sine_part, second * cosine + f...]
  transfers between devices with their start and end apart: 9 -> 0, of which waited for: 7 -> 0; matrix products, arithmetic and copies ran while one was open for 24% -> 0% of each run, Pallas kernels for 0% -> 0%
where the time goes in v1:
time: 49.6 us; the launch traced here: 49.4 us
  Pallas kernels  46 us (93%)
  local copies, waits for them, and re-layouts  3.38 us (7%)
    pallas_call x1, Pallas kernels, local(): pl.pallas_call(functools.partial(kernel, n_sp, chunks), out_shape=jax.Sha...  46 us
    unnamed x1, local copies, waits for them, and re-layouts  2.09 us
    reshape x1, local copies, waits for them, and re-layouts, local(): norm_gain.reshape(1, width)  1.29 us

profile of v1, /device:TPU:25, one launch (start us, length us, event | category | flops | bytes accessed | tf_op | source)
XLA Modules:
  0.0 49.4 jit_solution(5986875311988922278)
XLA Ops:
  0.0 1.3 %reshape.3.gain_ref = bf16[1,2048]{1,0:T(2,128)(2,1)} reshape(bf16[2048]{0:T(1024)(128)(2,1)} %param.18) | data formatting | bytes 8192 | tf_op jit(solution)/shard_map/reshape | solution.py:549
  1.3 46.0 %shard_map.163 = bf16[192,2048]{1,0:T(8,128)(2,1)} custom-call(bf16[768,2048]{1,0:T(8,128)(2,1)} %acts_hbm.1, bf16[1,2048]{1,0:T(2,128)(2,1)} %reshape.3.gain_ref, bf16[2048,256]{1,0:T(8,128)(2,1)} %wco_hbm.1, bf16[2048,256]{1,0:T(8,128)(2,1)} %wci_hbm.1, bf16[2048,256]{1,0:T(8,128)(2,1)} %wcv_hbm.1, bf16[3,256]{1,0:T(4,128)(2,1)} %taps_ref.1, ...), custom_call_target="tpu_custom_call" | custom-call | tf_op jit(solution)/shard_map/pallas_call | solution.py:503
  47.3 2.1 %copy.19 = bf16[192,2048]{1,0:T(8,128)(2,1)} copy(bf16[192,2048]{1,0:T(8,128)(2,1)} %shard_map.163) | data formatting | bytes 1572864

commit v2 on v1

--- a/solution.py
+++ b/solution.py
@@ -44,23 +44,31 @@
     n_sp,
     chunks,
     acts_hbm,
-    gain_ref,
+    gain_hbm,
     wco_hbm,
     wci_hbm,
     wcv_hbm,
-    taps_ref,
+    taps_hbm,
     wq_hbm,
     wk_hbm,
     wv_hbm,
     wg_hbm,
-    decay_ref,
+    decay_hbm,
     woc_hbm,
     wor_hbm,
+    cos_in_hbm,
+    sin_in_hbm,
+    cos_off_hbm,
+    sin_off_hbm,
+    own_out,
+    recv_b,
+    gain_ref,
+    taps_ref,
+    decay_ref,
     cos_in_ref,
     sin_in_ref,
     cos_off_ref,
     sin_off_ref,
-    out_ref,
     x_ref,
     w_ref,
     wo_ref,
@@ -87,7 +95,8 @@
     recv_a,
     own_ref,
     send_b,
-    recv_b,
+    small_sem,
+    out_sem,
     x_sem,
     w_sem,
     scan_send_sem,
@@ -103,15 +112,15 @@
     ch = co_ref.shape[1]
     rc = heads * HEAD
     blocks = rows // BLK
-    tiles = blocks
     proj = 256 if rows % 256 == 0 else BLK
+    tiles = rows // proj
     widths = windows_of(n_sp)
     distances = [d for w in widths for d in (w, 2 * w) if d < n_sp]
     sibling, across = tp ^ 1, tp ^ 2
 
     x_copies = [
         pltpu.make_async_copy(
-            acts_hbm.at[pl.ds(i * BLK, BLK)], x_ref.at[pl.ds(i * BLK, BLK)], x_sem.at[i]
+            acts_hbm.at[pl.ds(i * proj, proj)], x_ref.at[pl.ds(i * proj, proj)], x_sem.at[i]
         )
         for i in range(tiles)
     ]
@@ -136,9 +145,27 @@
         start += size
     w_copies["oc"] = pltpu.make_async_copy(woc_hbm, wo_ref.at[pl.ds(0, ch)], w_sem.at[7])
     w_copies["or"] = pltpu.make_async_copy(wor_hbm, wo_ref.at[pl.ds(ch, rc)], w_sem.at[8])
-    for copy in x_copies:
+    small = [
+        pltpu.make_async_copy(src, dst, small_sem.at[index])
+        for index, (src, dst) in enumerate(
+            (
+                (decay_hbm, decay_ref),
+                (gain_hbm, gain_ref),
+                (cos_off_hbm, cos_off_ref),
+                (sin_off_hbm, sin_off_ref),
+                (cos_in_hbm, cos_in_ref),
+                (sin_in_hbm, sin_in_ref),
+                (taps_hbm, taps_ref),
+            )
+        )
+    ]
+    for copy in small[:2] + x_copies[:1]:
         copy.start()
-    for name in ("k", "v", "q", "g", "ci", "cv", "co", "oc", "or"):
+    w_copies["k"].start()
+    w_copies["v"].start()
+    for copy in x_copies[1:] + small[2:]:
+        copy.start()
+    for name in ("q", "g", "ci", "cv", "co", "oc", "or"):
         w_copies[name].start()
 
     barrier = pltpu.get_barrier_semaphore()
@@ -160,13 +187,7 @@
             + jnp.where(sp >= d, jnp.int32(1), jnp.int32(0))
         )
 
-    for b in range(blocks):
-        c_off = cos_off_ref[pl.ds(sp * blocks + b, 1), :]
-        s_off = sin_off_ref[pl.ds(sp * blocks + b, 1), :]
-        c_in, s_in = cos_in_ref[...], sin_in_ref[...]
-        cs_ref[pl.ds(b * BLK, BLK), :] = c_off * c_in - s_off * s_in
-        sn_ref[pl.ds(b * BLK, BLK), :] = s_off * c_in + c_off * s_in
-
+    small[0].wait()
     ld_ref[...] = jnp.zeros_like(ld_ref)
     for h in range(heads):
         for b in range(blocks):
@@ -188,15 +209,26 @@
     key_scale = jnp.exp(rest_col)
     query_scale = jnp.exp(level_col)
 
-    def norm_tile(i, carry):
-        at = pl.ds(pl.multiple_of(i * BLK, BLK), BLK)
-        pltpu.make_async_copy(acts_hbm.at[at], x_ref.at[at], x_sem.at[i]).wait()
+    small[1].wait()
+    gain = gain_ref[...].astype(F32)[None, :]
+
+    def norm_tile(i):
+        at = slice(i * proj, (i + 1) * proj)
         x = x_ref[at, :].astype(F32)
         mean_sq = jnp.mean(x * x, axis=-1, keepdims=True)
-        x_ref[at, :] = (x * lax.rsqrt(mean_sq + EPS) * gain_ref[...].astype(F32)).astype(BF16)
-        return carry
-
-    lax.fori_loop(0, tiles, norm_tile, 0)
+        x_ref[at, :] = (x * lax.rsqrt(mean_sq + EPS) * gain).astype(BF16)
+
+    x_copies[0].wait()
+    norm_tile(0)
+
+    for copy in small[2:]:
+        copy.wait()
+    for b in range(blocks):
+        c_off = cos_off_ref[pl.ds(sp * blocks + b, 1), :]
+        s_off = sin_off_ref[pl.ds(sp * blocks + b, 1), :]
+        c_in, s_in = cos_in_ref[...], sin_in_ref[...]
+        cs_ref[pl.ds(b * BLK, BLK), :] = c_off * c_in - s_off * s_in
+        sn_ref[pl.ds(b * BLK, BLK), :] = s_off * c_in + c_off * s_in
 
     def project(at, first, last):
         lo, hi = bounds[first][0], bounds[last][1]
@@ -215,16 +247,16 @@
 
     w_copies["k"].wait()
     w_copies["v"].wait()
-
-    def kv_tile(i, carry):
-        at = tile_at(i)
+    for copy in x_copies[1:]:
+        copy.wait()
+    for i in range(tiles):
+        at = slice(i * proj, (i + 1) * proj)
         both = project(at, "k", "v")
+        if i + 1 < tiles:
+            norm_tile(i + 1)
         v_ref[at, :] = both[:, rc:]
         for h, turned in enumerate(rotate(both[:, :rc], at)):
             k_ref[at, h * HEAD : (h + 1) * HEAD] = turned
-        return carry
-
-    lax.fori_loop(0, rows // proj, kv_tile, 0)
 
     device_total = []
     starts = []
@@ -395,7 +427,7 @@
 
     w_copies["oc"].wait()
     w_copies["or"].wait()
-    part = out_ref.shape[0]
+    part = own_out.shape[0]
     wide = width // chunks
 
     def partial(block, c):
@@ -417,7 +449,7 @@
     def to_across(c):
         return pltpu.make_async_remote_copy(
             src_ref=send_b.at[c],
-            dst_ref=recv_b.at[c],
+            dst_ref=recv_b.at[:, pl.ds(c * wide, wide)],
             send_sem=b_sem.at[0, c],
             recv_sem=b_sem.at[1, c],
             device_id=(sp, across),
@@ -441,14 +473,17 @@
         send_across(c)
     for c in range(chunks):
         send_sibling(1, c)
+    outs = [
+        pltpu.make_async_copy(
+            own_ref.at[c], own_out.at[:, pl.ds(c * wide, wide)], out_sem.at[c]
+        )
+        for c in range(chunks)
+    ]
     for c in range(chunks):
-        own_ref[c] = partial(tp, c)
-    for c in range(chunks):
+        own = partial(tp, c)
         to_sibling(1, c).wait_recv()
-        own_ref[c] += recv_a[1, c].astype(F32)
-    for c in range(chunks):
-        to_across(c).wait_recv()
-        out_ref[:, c * wide : (c + 1) * wide] = (own_ref[c] + recv_b[c].astype(F32)).astype(BF16)
+        own_ref[c] = (own + recv_a[1, c].astype(F32)).astype(BF16)
+        outs[c].start()
 
     for r in range(len(widths)):
         for j in range(2):
@@ -466,7 +501,8 @@
     for c in range(chunks):
         to_sibling(0, c).wait_send()
         to_sibling(1, c).wait_send()
-        to_across(c).wait_send()
+        outs[c].wait()
+        to_across(c).wait()
 
 
 def local(
@@ -497,15 +533,21 @@
     rounds = len(windows_of(n_sp))
     pad = -(-heads * blocks // 8) * 8
     tables = [jnp.asarray(t) for t in rotary_tables(n_sp * blocks)]
-    vmem = pl.BlockSpec(memory_space=pltpu.VMEM)
     hbm = pl.BlockSpec(memory_space=pl.ANY)
     dma = pltpu.SemaphoreType.DMA
-    return pl.pallas_call(
+    own, received = pl.pallas_call(
         functools.partial(kernel, n_sp, chunks),
-        out_shape=jax.ShapeDtypeStruct((part, width), BF16),
-        in_specs=[hbm, vmem, hbm, hbm, hbm, vmem, hbm, hbm, hbm, hbm, vmem, hbm, hbm] + [vmem] * 4,
-        out_specs=vmem,
+        out_shape=[jax.ShapeDtypeStruct((part, width), BF16)] * 2,
+        in_specs=[hbm] * 17,
+        out_specs=[hbm] * 2,
         scratch_shapes=[
+            pltpu.VMEM(norm_gain.shape, BF16),
+            pltpu.VMEM(conv_taps.shape, BF16),
+            pltpu.VMEM(log_decay.shape, F32),
+            pltpu.VMEM((BLK, HEAD), F32),
+            pltpu.VMEM((BLK, HEAD), F32),
+            pltpu.VMEM((n_sp * blocks, HEAD), F32),
+            pltpu.VMEM((n_sp * blocks, HEAD), F32),
             pltpu.VMEM((rows, width), BF16),
             pltpu.VMEM((width, 3 * ch + 4 * rc), BF16),
             pltpu.VMEM((ch + rc, width), BF16),
@@ -530,9 +572,10 @@
             pltpu.VMEM((rounds, 2, 8, HEAD), F32),
             pltpu.VMEM((2, chunks, part, wide), BF16),
             pltpu.VMEM((2, chunks, part, wide), BF16),
-            pltpu.VMEM((chunks, part, wide), F32),
             pltpu.VMEM((chunks, part, wide), BF16),
             pltpu.VMEM((chunks, part, wide), BF16),
+            dma((7,)),
+            dma((chunks,)),
             dma((blocks,)),
             dma((9,)),
             dma((rounds, 2, 2)),
@@ -546,7 +589,7 @@
         ),
     )(
         activations,
-        norm_gain.reshape(1, width),
+        norm_gain,
         w_conv_outer,
         w_conv_inner,
         w_conv_value,
@@ -560,6 +603,7 @@
         w_out_ret,
         *tables,
     )
+    return (own.astype(F32) + received.astype(F32)).astype(BF16)
 
 
 def solution(mesh):

time: 49.6 us -> 46.4 us (0.935)
  local copies, waits for them, and re-layouts: 3.38 us -> 0 us
  other arithmetic: 0 us -> 2.52 us
  Pallas kernels: 46 us -> 43.8 us
    convert_element_type x0 -> x1, other arithmetic: none -> 2.52 us  [local(): return (own.astype(F32) + received.astype(F32)).astype(BF16)]
    pallas_call x1, Pallas kernels: 46 us -> 43.8 us  [local(): pl.pallas_call(functools.partial(kernel, n_sp, chunks), out_shape=[jax.Sh...]
    unnamed x1 -> x0, local copies, waits for them, and re-layouts: 2.09 us -> none
    reshape x1 -> x0, local copies, waits for them, and re-layouts: 1.29 us -> none  [local(): norm_gain.reshape(1, width)]
where the time goes in v2:
time: 46.4 us; the launch traced here: 46.3 us
  Pallas kernels  43.8 us (94%)
  other arithmetic  2.52 us (5%)
    pallas_call x1, Pallas kernels, local(): pl.pallas_call(functools.partial(kernel, n_sp, chunks), out_shape=[jax.Sh...  43.8 us
    convert_element_type x1, other arithmetic, local(): return (own.astype(F32) + received.astype(F32)).astype(BF16)  2.52 us

profile of v2, /device:TPU:25, one launch (start us, length us, event | category | flops | bytes accessed | tf_op | source)
XLA Modules:
  0.0 46.3 jit_solution(15830901546841463179)
XLA Ops:
  0.0 43.8 %shard_map.163 = (bf16[192,2048]{1,0:T(8,128)(2,1)}, bf16[192,2048]{1,0:T(8,128)(2,1)}) custom-call(bf16[768,2048]{1,0:T(8,128)(2,1)} %acts_hbm.1, bf16[2048]{0:T(1024)(128)(2,1)} %gain_hbm.1, bf16[2048,256]{1,0:T(8,128)(2,1)} %wco_hbm.1, bf16[2048,256]{1,0:T(8,128)(2,1)} %wci_hbm.1, bf16[2048,256]{1,0:T(8,128)(2,1)} %wcv_hbm.1, bf16[3,256]{1,0:T(4,128)(2,1)} %taps_hbm.1, ...), custom_call_target="tpu_custom_call" | custom-call | tf_op jit(solution)/shard_map/pallas_call | solution.py:538
  43.8 2.5 %add_convert_fusion = bf16[192,2048]{1,0:T(8,128)(2,1)} fusion(bf16[192,2048]{1,0:T(8,128)(2,1)} %get-tuple-element.8, bf16[192,2048]{1,0:T(8,128)(2,1)} %get-tuple-element.7), kind=kLoop, calls=%fused_computation | loop fusion | flops 1572864 | bytes 2359296 | tf_op jit(solution)/shard_map/convert_element_type | solution.py:606

commit v3 on v2

--- a/solution.py
+++ b/solution.py
@@ -313,7 +313,7 @@
                 state = state + jnp.exp(device_total[h]) * es_ref[cols, :]
             send_s[r, cols, :] = state.astype(BF16)
             send_l[r, h : h + 1, :] = device_total[h] + el_ref[h : h + 1, :]
-        for j in range(2):
+        for j in (1, 0):
             d = (j + 1) * widths[r]
             if d < n_sp:
                 @pl.when(sp + d < n_sp)
@@ -528,7 +528,7 @@
     ch = w_conv_outer.shape[1]
     rc = heads * HEAD
     part = rows // n_tp
-    chunks = 4
+    chunks = 8
     wide = width // chunks
     rounds = len(windows_of(n_sp))
     pad = -(-heads * blocks // 8) * 8

time: 46.4 us -> 47.1 us (1.015)
  the two profiles are of different devices: /device:TPU:25 before, /device:TPU:19 now
where the time goes in v3:
time: 47.1 us; the launch traced here: 47 us
  Pallas kernels  44.4 us (94%)
  other arithmetic  2.52 us (5%)
    pallas_call x1, Pallas kernels, local(): pl.pallas_call(functools.partial(kernel, n_sp, chunks), out_shape=[jax.Sh...  44.4 us
    convert_element_type x1, other arithmetic, local(): return (own.astype(F32) + received.astype(F32)).astype(BF16)  2.52 us

profile of v3, /device:TPU:19, one launch (start us, length us, event | category | flops | bytes accessed | tf_op | source)
XLA Modules:
  0.0 47.0 jit_solution(4211118470014284034)
XLA Ops:
  0.0 44.4 %shard_map.163 = (bf16[192,2048]{1,0:T(8,128)(2,1)}, bf16[192,2048]{1,0:T(8,128)(2,1)}) custom-call(bf16[768,2048]{1,0:T(8,128)(2,1)} %acts_hbm.1, bf16[2048]{0:T(1024)(128)(2,1)} %gain_hbm.1, bf16[2048,256]{1,0:T(8,128)(2,1)} %wco_hbm.1, bf16[2048,256]{1,0:T(8,128)(2,1)} %wci_hbm.1, bf16[2048,256]{1,0:T(8,128)(2,1)} %wcv_hbm.1, bf16[3,256]{1,0:T(4,128)(2,1)} %taps_hbm.1, ...), custom_call_target="tpu_custom_call" | custom-call | tf_op jit(solution)/shard_map/pallas_call | solution.py:538
  44.4 2.5 %add_convert_fusion = bf16[192,2048]{1,0:T(8,128)(2,1)} fusion(bf16[192,2048]{1,0:T(8,128)(2,1)} %get-tuple-element.8, bf16[192,2048]{1,0:T(8,128)(2,1)} %get-tuple-element.7), kind=kLoop, calls=%fused_computation | loop fusion | flops 1572864 | bytes 2359296 | tf_op jit(solution)/shard_map/convert_element_type | solution.py:606
